TPU v7x, 512 devices: a whole 4x4x16 slice. The times are simulated.
512 devices in a mesh: ep: 32 (over z, core), tp: 16 (over y, x).
Axes of the slice: x: 4, y: 4, z: 16, core: 2. Of those that a mesh axis runs over, the one named last changes fastest.
Arguments:
- tokens: bfloat16 [1024, 2048], P('ep', 'tp'), may hold values from -200 to 200
- routing: int32 [1024, 4], P('ep'), may hold values from 0 to 63, all different within a row; in each aligned block of 32 rows (0 to 31, 32 to 63, ...) at most 8 rows name the same one
- gate_weights: float32 [1024, 4], P('ep'), may hold values from 0.05 to 1
- norm_gain: float32 [2048], replicated, may hold values from 0.1 to 1.9
- w_gate: bfloat16 [64, 2048, 2048], P('ep', None, 'tp'), may hold values from -0.33007812 to 0.33007812
- w_up: bfloat16 [64, 2048, 2048], P('ep', None, 'tp'), may hold values from -0.33007812 to 0.33007812
- w_down: bfloat16 [64, 2048, 2048], P('ep', 'tp'), may hold values from -0.026489258 to 0.026489258
Outputs:
- mixed: bfloat16 [1024, 2048], P('ep', 'tp')
Inputs may be any that keep to these rules, and one draw needn't show every extreme that they name: `routing`: each token names 4 different experts. Among the 32 tokens of one index of ep no expert is named more than 8 times, a bound that some block reaches.
All inputs are finite; a program needn't handle non-finite values.
Results may differ from a plain program's by a relative error of at most 0.015.
Values may be sent and summed in bfloat16 or wider, within the bound.
A program may use at most 128 MiB of HBM per device.

v0:
```python
import jax
import jax.numpy as jnp
from jax import lax
from jax.sharding import PartitionSpec as P

D = 2048
CAP = 8
norm_eps = 1e-06
clamp_limit = 7.0
swish_alpha = 1.702


def activate(pre_gate, pre_up):
    clamped = jnp.minimum(pre_gate, clamp_limit)
    upper = jnp.clip(pre_up, -clamp_limit, clamp_limit)
    return (clamped * jax.nn.sigmoid(swish_alpha * clamped) * (upper + 1.0)).astype(jnp.bfloat16)


def per_device(tokens, routing, gate_weights, norm_gain, w_gate, w_up, w_down):
    ep_size = lax.axis_size("ep")
    exp_here = w_gate.shape[0]
    expert_count = exp_here * ep_size
    tok_rows = tokens.shape[0]
    top_count = routing.shape[1]
    col_width = tokens.shape[1]
    chosen = routing.reshape(-1)
    onehot = (chosen[:, None] == jnp.arange(expert_count, dtype=jnp.int32)[None, :]).astype(
        jnp.int32
    )
    slot_rank = jnp.sum(jnp.cumsum(onehot, axis=0) * onehot, axis=1) - 1
    slot_index = (chosen * CAP + slot_rank).reshape(tok_rows, top_count)
    slot_ids = jnp.arange(expert_count * CAP, dtype=jnp.int32)
    matches = slot_ids[:, None, None] == slot_index[None, :, :]
    placing = jnp.sum(matches.astype(jnp.float32), axis=2).astype(jnp.bfloat16)
    outgoing = jnp.dot(placing, tokens, preferred_element_type=jnp.float32).astype(jnp.bfloat16)
    outgoing = outgoing.reshape(ep_size, exp_here, CAP, col_width)
    received = lax.all_to_all(outgoing, "ep", split_axis=0, concat_axis=0, tiled=True)
    received = jnp.transpose(received, (1, 0, 2, 3)).reshape(exp_here, ep_size * CAP, col_width)
    raw = lax.all_gather(received, "tp", axis=2, tiled=True)
    wide = raw.astype(jnp.float32)
    ssq = jnp.sum(wide * wide, axis=2, keepdims=True)
    rows = (wide * lax.rsqrt(ssq / D + norm_eps) * norm_gain).astype(jnp.bfloat16)
    gate_part = jnp.einsum("erd,edf->erf", rows, w_gate, preferred_element_type=jnp.float32)
    up_part = jnp.einsum("erd,edf->erf", rows, w_up, preferred_element_type=jnp.float32)
    hidden = activate(gate_part, up_part)
    partial_value = jnp.einsum("erf,efd->erd", hidden, w_down, preferred_element_type=jnp.float32)
    summed = lax.psum_scatter(
        partial_value.astype(jnp.bfloat16), "tp", scatter_dimension=2, tiled=True
    )
    summed = jnp.transpose(summed.reshape(exp_here, ep_size, CAP, col_width), (1, 0, 2, 3))
    returned = lax.all_to_all(summed, "ep", split_axis=0, concat_axis=0, tiled=True)
    returned = returned.reshape(expert_count * CAP, col_width).astype(jnp.float32)
    combine = jnp.sum(matches.astype(jnp.float32) * gate_weights[None, :, :], axis=2)
    mixed = jnp.dot(combine.T, returned, precision=lax.Precision.HIGHEST)
    return mixed.astype(jnp.bfloat16)


def solution(mesh):
    placed = (
        P("ep", "tp"),
        P("ep", None),
        P("ep", None),
        P(),
        P("ep", None, "tp"),
        P("ep", None, "tp"),
        P("ep", "tp", None),
    )
    return jax.shard_map(
        per_device, mesh=mesh, in_specs=placed, out_specs=P("ep", "tp"), check_vma=False
    )
```

profile of v0, /device:TPU:1, one launch (start us, length us, event | category | flops | bytes accessed | tf_op | source)
XLA Modules:
  0.0 240.7 jit_solution(11151847588226632373)
XLA Ops:
  6.5 0.0 copy-start
  6.5 0.0 copy-start.2
  6.5 0.0 all-gather.2.cloned.1.call-start
  6.5 0.9 copy.42
  7.4 0.1 eq.29
  7.5 0.1 fusion.34
  7.6 0.2 reduce_window_sum.11
  7.8 0.2 select_reduce_fusion.1
  8.0 0.1 sub.7
  8.1 0.1 copy.43
  8.2 0.7 multiply_add_fusion
  8.8 0.8 convert_reduce_fusion
  9.7 0.9 convolution_convert_fusion.1
  10.6 32.4 %all_to_all.10 = bf16[32,2,8,128]{3,2,1,0:T(8,128)(2,1)S(1)} all-to-all(bf16[32,2,8,128]{3,2,1,0:T(8,128)(2,1)S(1)} %bitcast.24), channel_id=1, replica_groups=mesh['ep'=32,'tp'=16] {'ep'}, dimensions={0} | all-to-all | bytes 262144 | tf_op jit(solution)/shard_map/all_to_all | solution.py:37
  43.0 0.7 copy_bitcast_fusion
  43.6 0.0 all-gather.2.cloned.1.call-update
  43.6 0.0 reduce-scatter.4.cloned.1.call-start
  43.7 53.2 %all-gather.2.cloned.1.call-done = bf16[2,256,2048]{2,1,0:T(8,128)(2,1)} async-done(((bf16[2,256,128]{2,1,0:T(8,128)(2,1)}), bf16[2,256,2048]{2,1,0:T(8,128)(2,1)}) %all-gather.2.cloned.1.call-update) | async-done | bytes 2097168 | tf_op jit(solution)/shard_map/all_gather | solution.py:39
  96.9 0.0 copy-start.1
  96.9 2.2 fusion
  99.1 0.0 copy-done.2
  99.1 0.0 copy-done.1
  99.1 2.0 fusion.7
  101.2 0.0 copy-done
  101.2 4.0 %convolution_convert_fusion = bf16[2,256,2048]{2,1,0:T(8,128)(2,1)} fusion(bf16[2,128,2048]{2,1,0:T(8,128)(2,1)S(1)} %copy-done, bf16[2,2048,128]{2,1,0:T(8,128)(2,1)} %param.12, bf16[2,256,2048]{2,1,0:T(8,128)(2,1)S(1)} %copy-done.1, f32[2048]{0:T(1024)S(1)} %copy-done.2, f32[2,256]{1,0:T(2,128)S(1)} %add_rsqrt_fusion, f32[2,256,128]{2,1,0:T(8,128)S(1)} %fusion.7), kind=kOutput, calls=%fused_computation.5 | convolution fusion | flops 542703616 | bytes 6563840 | tf_op jit(solution)/shard_map/erf,efd->erd/dot_general | solution.py:46
  105.2 4.8 %copy.46 = bf16[2,256,2048]{1,0,2:T(2,128)(2,1)S(1)} copy(bf16[2,256,2048]{2,1,0:T(8,128)(2,1)} %convolution_convert_fusion) | data formatting | bytes 4194304
  110.0 1.8 copy.48
  111.8 0.0 reduce-scatter.4.cloned.1.call-update
  111.8 89.9 %reduce-scatter.4.cloned.1.call-done = bf16[128,512]{1,0:T(8,128)(2,1)} async-done(((bf16[2048,512]{1,0:T(8,128)(2,1)}), bf16[128,512]{1,0:T(8,128)(2,1)}) %reduce-scatter.4.cloned.1.call-update) | async-done | bytes 131088
  201.7 0.9 reshape.38
  202.6 0.1 copy.47
  202.8 30.3 %all_to_all.11 = bf16[32,2,8,128]{3,2,1,0:T(8,128)(2,1)S(1)} all-to-all(bf16[32,2,8,128]{3,2,1,0:T(8,128)(2,1)S(1)} %copy.45), channel_id=1, replica_groups=mesh['ep'=32,'tp'=16] {'ep'}, dimensions={0} | all-to-all | bytes 262144 | tf_op jit(solution)/shard_map/all_to_all | solution.py:51
  233.1 0.8 convolution_convert_fusion.2
  (3 shorter events, 0.0 us)
Async XLA Ops:
  6.5 94.6 %copy-start = (bf16[2,128,2048]{2,1,0:T(8,128)(2,1)S(1)}, bf16[2,128,2048]{2,1,0:T(8,128)(2,1)}, u32[]{:S(2)}) copy-start(bf16[2,128,2048]{2,1,0:T(8,128)(2,1)} %param.13) | copy-start | bytes 3145732
  6.5 92.6 %copy-start.2 = (f32[2048]{0:T(1024)S(1)}, f32[2048]{0:T(1024)}, u32[]{:S(2)}) copy-start(f32[2048]{0:T(1024)} %param.10) | copy-start | bytes 24580
  6.5 90.3 %all-gather.2.cloned.1.call-start = ((), (), s32[]{:S(2)}) async-start(), calls=%async_computation.3 | async-start | bytes 2228224 | tf_op jit(solution)/shard_map/all_gather | solution.py:39
  43.6 158.0 %reduce-scatter.4.cloned.1.call-start = ((), (), s32[]{:S(2)}) async-start(), calls=%async_computation.4 | async-start | bytes 2228224
  96.9 2.2 copy-start.1
Sparse Core Ops, SparseCore 0:
  43.8 53.0 all-gather.1
  112.0 89.6 reduce-scatter.3
where the time goes:
time: 241 us
  waiting for transfers between devices  143 us (59%)
  blocking collectives  62.7 us (26%)
  between operations  13.5 us (6%)
  local copies, waits for them, and re-layouts  9.54 us (4%)
  matrix products  7.72 us (3%)
  other arithmetic  4.16 us (2%)
    unnamed x3, waiting for transfers between devices  89.9 us
    all_gather x1, waiting for transfers between devices, per_device(): raw = lax.all_gather(received, 'tp', axis=2, tiled=True)  53.2 us
    all_to_all x1, blocking collectives, per_device(): lax.all_to_all(outgoing, 'ep', split_axis=0, concat_axis=0, tiled=True)  32.4 us
    all_to_all x1, blocking collectives, per_device(): lax.all_to_all(summed, 'ep', split_axis=0, concat_axis=0, tiled=True)  30.3 us
    unnamed x11, local copies, waits for them, and re-layouts  8.58 us
  transfers between devices with their start and end apart: 2, of which 2 were waited for; matrix products, arithmetic and copies ran while one was open for 0% of the time, Pallas kernels for 0%

commit v1 on v0

--- a/solution.py
+++ b/solution.py
@@ -36,7 +36,9 @@
     outgoing = outgoing.reshape(ep_size, exp_here, CAP, col_width)
     received = lax.all_to_all(outgoing, "ep", split_axis=0, concat_axis=0, tiled=True)
     received = jnp.transpose(received, (1, 0, 2, 3)).reshape(exp_here, ep_size * CAP, col_width)
-    raw = lax.all_gather(received, "tp", axis=2, tiled=True)
+    raw = jnp.concatenate(
+        lax.all_to_all(jnp.stack([received] * lax.axis_size("tp")), "tp", 0, 0), axis=2
+    )
     wide = raw.astype(jnp.float32)
     ssq = jnp.sum(wide * wide, axis=2, keepdims=True)
     rows = (wide * lax.rsqrt(ssq / D + norm_eps) * norm_gain).astype(jnp.bfloat16)

time: 241 us -> 214 us (0.89)
  waiting for transfers between devices: 143 us -> 80.1 us
  blocking collectives: 62.7 us -> 96.2 us
  local copies, waits for them, and re-layouts: 9.54 us -> 14.4 us
    all_gather x1 -> x0, waiting for transfers between devices: 53.2 us -> none  [per_device(): raw = lax.all_gather(received, 'tp', axis=2, tiled=True)]
    all_to_all x0 -> x1, blocking collectives: none -> 33.5 us  [per_device(): lax.all_to_all(jnp.stack([received] * lax.axis_size('tp')), 'tp', 0, 0)]
    unnamed x3 -> x2, waiting for transfers between devices: 89.9 us -> 80.1 us
    all_to_all x0 -> x2, local copies, waits for them, and re-layouts: none -> 2.86 us  [the longest x1 2.85 us: per_device(): lax.all_to_all(jnp.stack([received] * lax.axis_size('tp')), 'tp', 0, 0)]
    unnamed x11 -> x13, local copies, waits for them, and re-layouts: 8.58 us -> 10.8 us
  transfers between devices with their start and end apart: 2 -> 1, of which waited for: 2 -> 1; matrix products, arithmetic and copies ran while one was open for 0% -> 0% of each run, Pallas kernels for 0% -> 0%
where the time goes in v1:
time: 214 us; the launch traced here: 213 us
  blocking collectives  96.2 us (45%)
  waiting for transfers between devices  80.1 us (37%)
  local copies, waits for them, and re-layouts  14.4 us (7%)
  between operations  13.5 us (6%)
  matrix products  5.85 us (3%)
  other arithmetic  2.92 us (1%)
    unnamed x2, waiting for transfers between devices  80.1 us
    all_to_all x1, blocking collectives, per_device(): lax.all_to_all(jnp.stack([received] * lax.axis_size('tp')), 'tp', 0, 0)  33.5 us
    all_to_all x1, blocking collectives, per_device(): lax.all_to_all(outgoing, 'ep', split_axis=0, concat_axis=0, tiled=True)  32.4 us
    all_to_all x1, blocking collectives, per_device(): lax.all_to_all(summed, 'ep', split_axis=0, concat_axis=0, tiled=True)  30.3 us
    unnamed x13, local copies, waits for them, and re-layouts  10.8 us
  transfers between devices with their start and end apart: 1, of which 1 were waited for; matrix products, arithmetic and copies ran while one was open for 0% of the time, Pallas kernels for 0%

profile of v1, /device:TPU:1, one launch (start us, length us, event | category | flops | bytes accessed | tf_op | source)
XLA Modules:
  0.0 213.0 jit_solution(10194552313985877021)
XLA Ops:
  6.5 0.0 copy-start
  6.5 0.0 reduce-scatter.4.cloned.1.call-start
  6.5 0.8 copy.50
  7.4 0.1 eq.29
  7.5 0.1 fusion.15
  7.6 0.2 reduce_window_sum.11
  7.8 0.2 select_reduce_fusion.1
  8.0 0.1 sub.7
  8.1 0.1 copy.51
  8.1 0.7 multiply_add_fusion
  8.8 0.8 convert_reduce_fusion
  9.6 0.9 convolution_convert_fusion.1
  10.6 32.4 %all_to_all.15 = bf16[32,2,8,128]{3,2,1,0:T(8,128)(2,1)S(1)} all-to-all(bf16[32,2,8,128]{3,2,1,0:T(8,128)(2,1)S(1)} %bitcast.35), channel_id=1, replica_groups=mesh['ep'=32,'tp'=16] {'ep'}, dimensions={0} | all-to-all | bytes 262144 | tf_op jit(solution)/shard_map/all_to_all | solution.py:37
  43.0 0.5 stack.3
  43.4 33.5 %all_to_all.16 = bf16[16,2,256,128]{3,2,1,0:T(8,128)(2,1)} all-to-all(bf16[16,2,256,128]{3,2,1,0:T(8,128)(2,1)S(1)} %stack.3), channel_id=1, replica_groups=mesh['ep'=32,'tp'=16] {'tp'}, dimensions={0} | all-to-all | bytes 4194304 | tf_op jit(solution)/shard_map/all_to_all | solution.py:40
  77.0 2.9 %copy.53 = bf16[16,2,256,128]{2,3,0,1:T(8,128)(2,1)S(1)} copy(bf16[16,2,256,128]{3,2,1,0:T(8,128)(2,1)} %all_to_all.16) | data formatting | bytes 4194304 | tf_op jit(solution)/shard_map/all_to_all | solution.py:40
  79.8 0.0 copy-start.3
  79.8 0.5 multiply_reduce_fusion
  80.3 0.2 copy-done.3
  80.5 0.0 copy-start.2
  80.5 0.5 fusion.1
  81.0 0.0 copy-start.1
  81.0 1.3 copy-done.1
  82.4 0.0 copy-done.2
  82.4 0.9 convolution_minimum_fusion
  83.3 0.0 copy-done
  83.3 3.2 %convolution_convert_fusion = bf16[2,256,2048]{2,1,0:T(8,128)(2,1)S(1)} fusion(bf16[2,128,2048]{2,1,0:T(8,128)(2,1)S(1)} %copy-done, bf16[2,256,2048]{1,2,0:T(8,128)(2,1)} %copy-done.1, bf16[2,2048,128]{2,1,0:T(8,128)(2,1)} %param.12, f32[2,256,128]{2,1,0:T(8,128)S(1)} %convolution_minimum_fusion), kind=kOutput, calls=%fused_computation.4 | convolution fusion | flops 538509312 | bytes 6553600 | tf_op jit(solution)/shard_map/erf,efd->erd/dot_general | solution.py:48
  86.6 3.9 %copy.59 = bf16[2,256,2048]{1,0,2:T(2,128)(2,1)} copy(bf16[2,256,2048]{2,1,0:T(8,128)(2,1)S(1)} %convolution_convert_fusion) | data formatting | bytes 4194304
  90.5 3.4 %copy.61 = bf16[256,8,2,256]{3,1,2,0:T(8,128)(2,1)} copy(bf16[256,8,2,256]{3,2,1,0:T(2,128)(2,1)} %bitcast.32) | data formatting | bytes 4194304
  93.8 0.0 reduce-scatter.4.cloned.1.call-update
  93.9 80.1 %reduce-scatter.4.cloned.1.call-done = bf16[128,512]{1,0:T(8,128)(2,1)} async-done(((bf16[2048,512]{1,0:T(8,128)(2,1)}), bf16[128,512]{1,0:T(8,128)(2,1)}) %reduce-scatter.4.cloned.1.call-update) | async-done | bytes 131088
  174.0 0.9 reshape.41
  174.9 0.1 copy.60
  175.1 30.3 %all_to_all.17 = bf16[32,2,8,128]{3,2,1,0:T(8,128)(2,1)S(1)} all-to-all(bf16[32,2,8,128]{3,2,1,0:T(8,128)(2,1)S(1)} %copy.56), channel_id=1, replica_groups=mesh['ep'=32,'tp'=16] {'ep'}, dimensions={0} | all-to-all | bytes 262144 | tf_op jit(solution)/shard_map/all_to_all | solution.py:53
  205.4 0.8 convolution_convert_fusion.2
  (4 shorter events, 0.0 us)
Async XLA Ops:
  6.5 76.8 %copy-start = (bf16[2,128,2048]{2,1,0:T(8,128)(2,1)S(1)}, bf16[2,128,2048]{2,1,0:T(8,128)(2,1)}, u32[]{:S(2)}) copy-start(bf16[2,128,2048]{2,1,0:T(8,128)(2,1)} %param.13) | copy-start | bytes 3145732
  6.5 167.4 %reduce-scatter.4.cloned.1.call-start = ((), (), s32[]{:S(2)}) async-start(), calls=%async_computation.4 | async-start | bytes 2228224
  79.8 0.7 copy-start.3
  80.5 1.9 copy-start.2
  81.0 1.4 copy-start.1
Sparse Core Ops, SparseCore 0:
  94.0 79.9 reduce-scatter.3
